TPU v7x, 32 devices: a whole 2x2x4 slice. The times are simulated.
32 devices in a mesh: grp: 1, sp: 8 (over z, core), tp: 4 (over y, x).
Axes of the slice: x: 2, y: 2, z: 4, core: 2. Of those that a mesh axis runs over, the one named last changes fastest.
Arguments:
- queries: bfloat16 [2048, 16, 128], P(('grp', 'sp'), 'tp'), may hold values from -6 to 6
- keys: bfloat16 [2048, 4, 128], P(('grp', 'sp'), 'tp'), may hold values from -6 to 6
- values: bfloat16 [2048, 4, 128], P(('grp', 'sp'), 'tp'), may hold values from -6 to 6
- log_gates: float32 [16, 2048], P('tp', ('grp', 'sp')), may hold values from -260 to 0, as said below
- documents: int32 [2048], P(('grp', 'sp')), may hold values from 0 to 2, never falling along the last dimension, each value on 1 to 1536 neighbouring positions
- query_gain: float32 [128], replicated, may hold values from 0.5 to 5
- key_gain: float32 [128], replicated, may hold values from 0.5 to 5
- out_weight: bfloat16 [2048, 2048], P('tp'), may hold values from -0.125 to 0.125
- residual: bfloat16 [2048, 2048], P(('grp', 'sp', 'tp')), may hold values from -1.5 to 1.5
- norm_gain: float32 [2048], replicated, may hold values from 0.1 to 1.9
- routes: int32 [2048, 2], P(('grp', 'sp', 'tp')), may hold values from 0 to 3, all different within a row; in each aligned block of 64 rows (0 to 63, 64 to 127, ...) at most 48 rows name the same one
- route_weights: float32 [2048, 2], P(('grp', 'sp', 'tp')), may hold values from 0.1 to 1
- w_gate: bfloat16 [8, 2048, 2048], P('sp', None, 'tp'), may hold values from -0.125 to 0.125
- w_up: bfloat16 [8, 2048, 2048], P('sp', None, 'tp'), may hold values from -0.125 to 0.125
- w_down: bfloat16 [8, 2048, 2048], P('sp', 'tp'), may hold values from -0.09375 to 0.09375
Outputs:
- layer_out: bfloat16 [2048, 2048], P(('grp', 'sp', 'tp'))
Inputs may be any that keep to these rules, and one draw needn't show every extreme that they name: `log_gates`: non-increasing along positions for every head. `documents`: never falls along positions. `routes`: the 2 experts of a token differ; among the 64 tokens of one device (aligned blocks) no expert is named by more than 48 tokens, and in every draw some expert is named by exactly 48 of them.
All inputs are finite; a program needn't handle non-finite values.
Results may differ from a plain program's by a relative error of at most 0.017.
The roundings to bfloat16 on the way count: a program that leaves them out, or rounds other values in their place, can miss the bound.
Values may be sent and summed in bfloat16 or wider, within the bound.
A program may use at most 128 MiB of HBM per device.

v0:
```python
import jax
import jax.numpy as jnp
from jax import lax
from jax.sharding import PartitionSpec as P

EPSILON = 1e-06
FLOOR = -1e30


def rms_scale(inputs, gain):
    return inputs * lax.rsqrt(jnp.mean(inputs * inputs, axis=-1, keepdims=True) + EPSILON) * gain


def local(
    queries,
    keys,
    values,
    log_gates,
    documents,
    query_gain,
    key_gain,
    out_weight,
    residual,
    norm_gain,
    routes,
    route_weights,
    w_gate,
    w_up,
    w_down,
):
    tok_dev, local_heads, head_size = queries.shape
    seq_index = lax.axis_index("sp")
    offset = seq_index * tok_dev
    query_norm = (rms_scale(queries.astype(jnp.float32), query_gain) * head_size ** (-0.5)).astype(
        jnp.bfloat16
    )
    key_norm = rms_scale(keys[:, 0, :].astype(jnp.float32), key_gain).astype(jnp.bfloat16)
    value_rows = values[:, 0, :]
    doc_float = documents.astype(jnp.float32)
    gates_all, docs_all = (
        lax.all_gather(log_gates, "sp", axis=1, tiled=True),
        lax.all_gather(doc_float[None, :], "sp", axis=1, tiled=True),
    )
    query_pos = offset + jnp.arange(tok_dev, dtype=jnp.int32)
    first_doc = doc_float[0]
    last_pos = offset + tok_dev - 1
    start_state = (
        jnp.full((local_heads, tok_dev), FLOOR, jnp.float32),
        jnp.zeros((local_heads, tok_dev), jnp.float32),
        jnp.zeros((local_heads, tok_dev, head_size), jnp.float32),
    )
    key_piece = lax.all_gather(key_norm, "sp", axis=0, tiled=True)
    value_piece = lax.all_gather(value_rows, "sp", axis=0, tiled=True)
    piece_rows = key_piece.shape[0]
    block_rows = 512
    block_count = piece_rows // block_rows

    def one_block(running, block_index):
        local_start = block_index * block_rows
        block_keys = lax.dynamic_slice_in_dim(key_piece, local_start, block_rows, 0)
        block_values = lax.dynamic_slice_in_dim(value_piece, local_start, block_rows, 0)
        block_gates = lax.dynamic_slice_in_dim(gates_all, local_start, block_rows, 1)
        block_docs = lax.dynamic_slice_in_dim(docs_all, local_start, block_rows, 1)[0]
        needed = (local_start <= last_pos) & (block_docs[block_rows - 1] >= first_doc)

        def update(current):
            running_max, running_sum, running_out = current
            scores = jnp.einsum(
                "qhd,kd->hqk", query_norm, block_keys, preferred_element_type=jnp.float32
            )
            scores = scores + log_gates[:, :, None] - block_gates[:, None, :]
            key_pos = local_start + jnp.arange(block_rows, dtype=jnp.int32)
            allowed = (key_pos[None, :] <= query_pos[:, None]) & (
                block_docs[None, :] == doc_float[:, None]
            )
            scores = jnp.where(allowed[None], scores, -jnp.inf)
            new_max = jnp.maximum(running_max, jnp.max(scores, axis=-1))
            expo = jnp.exp(scores - new_max[..., None])
            factor = jnp.exp(running_max - new_max)
            new_sum = factor * running_sum + jnp.sum(expo, axis=-1)
            added = jnp.einsum(
                "hqk,kd->hqd",
                expo.astype(jnp.bfloat16),
                block_values,
                preferred_element_type=jnp.float32,
            )
            return (new_max, new_sum, factor[..., None] * running_out + added)

        def keep(current):
            return current

        return (lax.cond(needed, update, keep, running), None)

    result, _ = lax.scan(one_block, start_state, jnp.arange(block_count, dtype=jnp.int32))
    final_max, final_sum, final_out = result
    attended = (final_out / final_sum[..., None]).astype(jnp.bfloat16)
    attended = jnp.transpose(attended, (1, 0, 2)).reshape(tok_dev, local_heads * head_size)
    n_sp = lax.axis_size("sp")
    n_tp = lax.axis_size("tp")
    rows_dev = tok_dev // n_tp
    projected = lax.psum_scatter(
        jnp.dot(attended, out_weight, preferred_element_type=jnp.float32).astype(jnp.bfloat16),
        "tp",
        scatter_dimension=0,
        tiled=True,
    ).astype(jnp.float32)
    mixed = (residual.astype(jnp.float32) + projected).astype(jnp.bfloat16)
    normed = rms_scale(mixed.astype(jnp.float32), norm_gain).astype(jnp.bfloat16)
    model_dim = normed.shape[1]
    experts = n_sp // 2
    capacity = min(rows_dev, 6 * rows_dev // n_sp)
    expert_ids = jnp.arange(experts, dtype=jnp.int32)
    chosen = routes[:, :, None] == expert_ids[None, None, :]
    picked = jnp.sum(chosen.astype(jnp.float32), axis=1)
    weight_of = jnp.sum(jnp.where(chosen, route_weights[:, :, None], 0.0), axis=1)
    rank = jnp.cumsum(picked, axis=0) - 1.0
    slot_ids = jnp.arange(capacity).astype(jnp.float32)
    placing = picked.T[:, None, :] * (rank.T[:, None, :] == slot_ids[None, :, None]).astype(
        jnp.float32
    )
    outgoing = jnp.einsum(
        "ecr,rd->ecd", placing.astype(jnp.bfloat16), normed, preferred_element_type=jnp.float32
    ).astype(jnp.bfloat16)
    outgoing = jnp.repeat(outgoing, 2, axis=0)
    gate_rows = w_gate[0]
    up_rows = w_up[0]
    down_rows = w_down[0]
    arrived = lax.all_gather(
        lax.all_to_all(outgoing, "sp", split_axis=0, concat_axis=0, tiled=True),
        "tp",
        axis=0,
        tiled=True,
    )
    lead, items, width = arrived.shape
    flat = arrived.reshape(lead * items, width)
    gate_act = jnp.dot(flat, gate_rows, preferred_element_type=jnp.float32)
    up_act = jnp.dot(flat, up_rows, preferred_element_type=jnp.float32)
    hidden = (jax.nn.silu(gate_act) * up_act).astype(jnp.bfloat16)
    partial_out = jnp.dot(hidden, down_rows, preferred_element_type=jnp.float32).astype(
        jnp.bfloat16
    )
    partial_all = partial_out.reshape(lead, items, width)
    summed = lax.psum_scatter(
        partial_all.astype(jnp.float32).astype(jnp.bfloat16), "tp", scatter_dimension=0, tiled=True
    ).astype(jnp.float32)
    returned = lax.all_to_all(
        summed.astype(jnp.bfloat16), "sp", split_axis=0, concat_axis=0, tiled=True
    ).astype(summed.dtype)
    results = jnp.sum(returned.reshape(experts, 2, capacity, model_dim), axis=1)
    combining = placing * weight_of.T[:, None, :]
    routed = jnp.einsum("ecr,ecd->rd", combining, results, precision=lax.Precision.HIGHEST)
    return (mixed.astype(jnp.float32) + routed).astype(jnp.bfloat16)


def solution(mesh):
    return jax.shard_map(
        local,
        mesh=mesh,
        in_specs=(
            P(("grp", "sp"), "tp", None),
            P(("grp", "sp"), "tp", None),
            P(("grp", "sp"), "tp", None),
            P("tp", ("grp", "sp")),
            P(("grp", "sp")),
            P(),
            P(),
            P("tp", None),
            P(("grp", "sp", "tp"), None),
            P(),
            P(("grp", "sp", "tp"), None),
            P(("grp", "sp", "tp"), None),
            P("sp", None, "tp"),
            P("sp", None, "tp"),
            P("sp", "tp", None),
        ),
        out_specs=P(("grp", "sp", "tp"), None),
        check_vma=False,
    )
```

profile of v0, /device:TPU:0, one launch (start us, length us, event | category | flops | bytes accessed | tf_op | source)
XLA Modules:
  0.0 380.4 jit_solution(16620844591719439829)
XLA Ops:
  6.5 0.0 copy-start
  6.5 0.0 copy-start.4
  6.5 0.0 reduce-scatter.3.cloned.1.call-start
  6.5 0.8 convert_element_type.80
  7.4 0.6 slice.7
  8.0 0.9 fusion.34
  8.9 1.2 fusion.23
  10.1 13.5 %all-gather.2 = f32[8,1,256]{2,1,0:T(1,128)S(1)} all-gather(f32[1,1,256]{2,1,0:T(1,128)S(1)} %bitcast.73), channel_id=2, replica_groups=mesh['grp'=1,'sp'=8,'tp'=4] {'sp'}, dimensions={0}, use_global_device_ids=true | all-gather | bytes 9216 | tf_op jit(solution)/shard_map/all_gather | solution.py:42
  23.6 14.2 %all_gather.17 = f32[4,2048]{1,0:T(4,128)S(1)} all-gather(f32[4,256]{1,0:T(4,128)} %param.22), channel_id=1, replica_groups=mesh['grp'=1,'sp'=8,'tp'=4] {'sp'}, dimensions={1}, use_global_device_ids=true | all-gather | bytes 36864 | tf_op jit(solution)/shard_map/all_gather | solution.py:41
  37.8 0.9 fusion.36
  38.8 15.8 %all_gather.16 = bf16[2048,128]{1,0:T(8,128)(2,1)} all-gather(bf16[256,128]{1,0:T(8,128)(2,1)S(1)} %fusion.36), channel_id=1, replica_groups=mesh['grp'=1,'sp'=8,'tp'=4] {'sp'}, dimensions={0}, use_global_device_ids=true | all-gather | bytes 589824 | tf_op jit(solution)/shard_map/all_gather | solution.py:52
  54.6 15.1 %all-gather.1 = bf16[2048,1,128]{2,0,1:T(8,128)(2,1)S(1)} all-gather(bf16[256,1,128]{2,0,1:T(8,128)(2,1)} %param.21), channel_id=3, replica_groups=mesh['grp'=1,'sp'=8,'tp'=4] {'sp'}, dimensions={0}, use_global_device_ids=true | all-gather | bytes 589824 | tf_op jit(solution)/shard_map/all_gather | solution.py:53
  69.7 1.2 fusion.26
  70.9 0.0 copy-done.4
  70.9 15.6 %while.15 = (s32[]{:T(128)}, f32[4,256]{1,0:T(4,128)S(1)}, f32[4,256]{1,0:T(4,128)S(1)}, f32[4,256,128]{2,1,0:T(8,128)S(1)}, s32[4]{0:T(128)S(1)}, /*index=5*/s3...) while((s32[]{:T(128)}, f32[4,256]{1,0:T(4,128)S(1)}, ...), condition=%wide.region_7.8_spmd.clone, body=%wide.region_2.7_spmd.clone.sunk | while | flops 273287936 | bytes 8237029 | solution.py:94
  70.9 0.7 dynamic_slice.48
  72.3 0.6 constant_dynamic-slice_fusion.5
  74.1 2.9 conditional.3
  74.1 0.1 constant_dynamic-slice_fusion
  74.2 0.2 compare_and_fusion
  74.4 1.5 fusion.49
  75.9 0.3 fusion.5
  76.2 0.7 convolution_add_fusion
  77.0 0.7 dynamic_slice.48
  78.3 0.6 constant_dynamic-slice_fusion.5
  80.2 0.7 dynamic_slice.48
  81.5 0.6 constant_dynamic-slice_fusion.5
  83.4 0.7 dynamic_slice.48
  84.7 0.6 constant_dynamic-slice_fusion.5
  86.6 0.2 copy.38
  86.8 0.0 copy-start.5
  86.8 0.0 copy-start.6
  86.8 0.0 copy-start.1
  86.8 0.0 copy-start.3
  86.9 3.4 convolution_convert_fusion.1
  90.2 0.0 reduce-scatter.3.cloned.1.call-update
  90.2 0.0 all-gather.5.cloned.1.call-start
  90.3 0.0 copy-done.5
  90.3 0.0 copy-done.6
  90.3 0.1 copy.39
  90.4 0.1 reduce_window_sum.11
  90.5 0.1 copy.40
  90.6 34.4 %reduce-scatter.3.cloned.1.call-done = bf16[64,2048]{1,0:T(8,128)(2,1)} async-done(((bf16[256,2048]{1,0:T(8,128)(2,1)}), bf16[64,2048]{1,0:T(8,128)(2,1)}) %reduce-scatter.3.cloned.1.call-update) | async-done | bytes 262160 | tf_op jit(solution)/shard_map/reduce_scatter | solution.py:101
  125.0 0.0 copy-done.1
  125.0 1.1 fusion.27
  126.1 0.0 copy-done.3
  126.2 1.4 convolution_convert_fusion.2
  127.5 0.2 broadcast_in_dim.72
  127.7 42.3 %all_to_all.10 = bf16[8,48,2048]{2,1,0:T(8,128)(2,1)} all-to-all(bf16[8,48,2048]{2,1,0:T(8,128)(2,1)S(1)} %bitcast.69), channel_id=1, replica_groups=mesh['grp'=1,'sp'=8,'tp'=4] {'sp'}, dimensions={0} | all-to-all | bytes 3145728 | tf_op jit(solution)/shard_map/all_to_all | solution.py:129
  170.0 0.0 all-gather.5.cloned.1.call-update
  170.1 0.0 reduce-scatter.5.cloned.1.call-start
  170.1 68.1 %all-gather.5.cloned.1.call-done = bf16[32,48,2048]{2,1,0:T(8,128)(2,1)} async-done(((bf16[8,48,2048]{2,1,0:T(8,128)(2,1)}), bf16[32,48,2048]{2,1,0:T(8,128)(2,1)}) %all-gather.5.cloned.1.call-update) | async-done | bytes 6291472 | tf_op jit(solution)/shard_map/all_gather | solution.py:128
  238.2 8.5 %fusion.19 = f32[1536,512]{1,0:T(8,128)} fusion(bf16[1536,2048]{1,0:T(8,128)(2,1)} %bitcast.78, bf16[1,2048,512]{2,1,0:T(8,128)(2,1)} %param.31), kind=kOutput, calls=%fused_computation.34 | convolution fusion | flops 3221225472 | bytes 11534336 | tf_op jit(solution)/shard_map/dot_general | solution.py:136
  246.7 0.0 copy-done
  246.7 11.8 %convolution_convert_fusion = bf16[1536,2048]{1,0:T(8,128)(2,1)} fusion(bf16[1,512,2048]{2,1,0:T(8,128)(2,1)S(1)} %copy-done, bf16[1536,2048]{1,0:T(8,128)(2,1)} %bitcast.79, f32[1536,512]{1,0:T(8,128)} %fusion.19, bf16[1,2048,512]{2,1,0:T(8,128)(2,1)} %param.32), kind=kOutput, calls=%fused_computation.23 | convolution fusion | flops 6450315264 | bytes 19922944 | tf_op jit(solution)/shard_map/dot_general | solution.py:139
  258.5 0.0 reduce-scatter.5.cloned.1.call-update
  258.5 70.1 %reduce-scatter.5.cloned.1.call-done = bf16[8,48,2048]{2,1,0:T(8,128)(2,1)} async-done(((bf16[32,48,2048]{2,1,0:T(8,128)(2,1)}), bf16[8,48,2048]{2,1,0:T(8,128)(2,1)}) %reduce-scatter.5.cloned.1.call-update) | async-done | bytes 1572880 | tf_op jit(solution)/shard_map/reduce_scatter | solution.py:143
  328.7 42.4 %all_to_all.11 = bf16[8,48,2048]{2,1,0:T(8,128)(2,1)S(1)} all-to-all(bf16[8,48,2048]{2,1,0:T(8,128)(2,1)} %reduce-scatter.5.cloned.1.call-done), channel_id=1, replica_groups=mesh['grp'=1,'sp'=8,'tp'=4] {'sp'}, dimensions={0} | all-to-all | bytes 3145728 | tf_op jit(solution)/shard_map/all_to_all | solution.py:146
  371.1 0.0 copy-start.2
  371.1 0.3 convert_reduce_fusion
  371.4 0.6 copy-done.2
  372.0 1.9 fusion.16
  (27 shorter events, 0.3 us)
Async XLA Ops:
  6.5 240.2 %copy-start = (bf16[1,512,2048]{2,1,0:T(8,128)(2,1)S(1)}, bf16[1,512,2048]{2,1,0:T(8,128)(2,1)}, u32[]{:S(2)}) copy-start(bf16[1,512,2048]{2,1,0:T(8,128)(2,1)} %param.33) | copy-start | bytes 6291460
  6.5 64.4 %copy-start.4 = (f32[4,256]{1,0:T(4,128)S(1)}, f32[4,256]{1,0:T(4,128)}, u32[]{:S(2)}) copy-start(f32[4,256]{1,0:T(4,128)} %param.22) | copy-start | bytes 12292
  6.5 118.4 %reduce-scatter.3.cloned.1.call-start = ((), (), s32[]{:S(2)}) async-start(), calls=%async_computation.4 | async-start | bytes 1310720 | tf_op jit(solution)/shard_map/reduce_scatter | solution.py:101
  86.8 3.5 copy-start.5
  86.8 3.5 copy-start.6
  86.8 38.2 %copy-start.1 = (bf16[64,2048]{1,0:T(8,128)(2,1)S(1)}, bf16[64,2048]{1,0:T(8,128)(2,1)}, u32[]{:S(2)}) copy-start(bf16[64,2048]{1,0:T(8,128)(2,1)} %param.27) | copy-start | bytes 786436
  86.8 39.3 %copy-start.3 = (f32[2048]{0:T(1024)S(1)}, f32[2048]{0:T(1024)}, u32[]{:S(2)}) copy-start(f32[2048]{0:T(1024)} %param.28) | copy-start | bytes 24580
  90.2 147.9 %all-gather.5.cloned.1.call-start = ((), (), s32[]{:S(2)}) async-start(), calls=%async_computation.5 | async-start | bytes 7864320 | tf_op jit(solution)/shard_map/all_gather | solution.py:128
  170.1 158.6 %reduce-scatter.5.cloned.1.call-start = ((), (), s32[]{:S(2)}) async-start(), calls=%async_computation.6 | async-start | bytes 7864320 | tf_op jit(solution)/shard_map/reduce_scatter | solution.py:143
  371.1 1.0 copy-start.2
Sparse Core Ops, SparseCore 0:
  90.4 34.5 reduce-scatter.2
  170.2 67.9 all-gather.4
  258.6 69.9 reduce-scatter.4
where the time goes:
time: 381 us; the launch traced here: 380 us
  waiting for transfers between devices  173 us (45%)
  blocking collectives  143 us (38%)
  matrix products  29.1 us (8%)
  between operations  13.3 us (3%)
  loops' own time  7.86 us (2%)
  other arithmetic  7.23 us (2%)
  local copies, waits for them, and re-layouts  6.88 us (2%)
    reduce_scatter x1, waiting for transfers between devices, local(): lax.psum_scatter(partial_all.astype(jnp.float32).astype(jnp.bfloat16), 't...  70.1 us
    all_gather x1, waiting for transfers between devices, local(): lax.all_gather(lax.all_to_all(outgoing, 'sp', split_axis=0, concat_axis=0...  68.1 us
    all_to_all x1, blocking collectives, local(): lax.all_to_all(summed.astype(jnp.bfloat16), 'sp', split_axis=0, concat_ax...  42.4 us
    all_to_all x1, blocking collectives, local(): lax.all_to_all(outgoing, 'sp', split_axis=0, concat_axis=0, tiled=True)  42.3 us
    reduce_scatter x1, waiting for transfers between devices, local(): lax.psum_scatter(jnp.dot(attended, out_weight, preferred_element_type=jnp...  34.4 us
    all_gather x1, blocking collectives, local(): key_piece = lax.all_gather(key_norm, 'sp', axis=0, tiled=True)  15.8 us
    all_gather x1, blocking collectives, local(): value_piece = lax.all_gather(value_rows, 'sp', axis=0, tiled=True)  15.1 us
    all_gather x1, blocking collectives, local(): lax.all_gather(log_gates, 'sp', axis=1, tiled=True)  14.2 us
  transfers between devices with their start and end apart: 3, of which 3 were waited for; matrix products, arithmetic and copies ran while one was open for 0% of the time, Pallas kernels for 0%

commit v1 on v0

--- a/solution.py
+++ b/solution.py
@@ -49,8 +49,11 @@
         jnp.zeros((local_heads, tok_dev), jnp.float32),
         jnp.zeros((local_heads, tok_dev, head_size), jnp.float32),
     )
-    key_piece = lax.all_gather(key_norm, "sp", axis=0, tiled=True)
-    value_piece = lax.all_gather(value_rows, "sp", axis=0, tiled=True)
+    key_piece, value_piece = jnp.split(
+        lax.all_gather(jnp.concatenate([key_norm, value_rows], axis=1), "sp", axis=0, tiled=True),
+        [key_norm.shape[1]],
+        axis=1,
+    )
     piece_rows = key_piece.shape[0]
     block_rows = 512
     block_count = piece_rows // block_rows

time: 381 us -> 353 us (0.927)
  blocking collectives: 143 us -> 112 us
    all_gather x2 -> x0, blocking collectives: 30.9 us -> none  [the longest x1 15.8 us: local(): key_piece = lax.all_gather(key_norm, 'sp', axis=0, tiled=True)]
  transfers between devices with their start and end apart: 3 -> 4, of which waited for: 3 -> 3; matrix products, arithmetic and copies ran while one was open for 0% -> 1% of each run, Pallas kernels for 0% -> 0%
where the time goes in v1:
time: 353 us
  waiting for transfers between devices  173 us (49%)
  blocking collectives  112 us (32%)
  matrix products  29.1 us (8%)
  between operations  13.3 us (4%)
  other arithmetic  8.75 us (2%)
  local copies, waits for them, and re-layouts  8.66 us (2%)
  loops' own time  7.76 us (2%)
    reduce_scatter x1, waiting for transfers between devices, local(): lax.psum_scatter(partial_all.astype(jnp.float32).astype(jnp.bfloat16), 't...  70.2 us
    all_gather x1, waiting for transfers between devices, local(): lax.all_gather(lax.all_to_all(outgoing, 'sp', split_axis=0, concat_axis=0...  68.1 us
    all_to_all x1, blocking collectives, local(): lax.all_to_all(summed.astype(jnp.bfloat16), 'sp', split_axis=0, concat_ax...  42.4 us
    all_to_all x1, blocking collectives, local(): lax.all_to_all(outgoing, 'sp', split_axis=0, concat_axis=0, tiled=True)  42.3 us
    reduce_scatter x1, waiting for transfers between devices, local(): lax.psum_scatter(jnp.dot(attended, out_weight, preferred_element_type=jnp...  34.3 us
    all_gather x1, blocking collectives, local(): lax.all_gather(log_gates, 'sp', axis=1, tiled=True)  14.2 us
    all_gather x1, blocking collectives, local(): lax.all_gather(doc_float[None, :], 'sp', axis=1, tiled=True)  13.5 us
    dot_general x1, matrix products, local(): jnp.dot(hidden, down_rows, preferred_element_type=jnp.float32)  11.7 us
  transfers between devices with their start and end apart: 4, of which 3 were waited for; matrix products, arithmetic and copies ran while one was open for 1% of the time, Pallas kernels for 0%

profile of v1, /device:TPU:0, one launch (start us, length us, event | category | flops | bytes accessed | tf_op | source)
XLA Modules:
  0.0 352.8 jit_solution(7900858133861365881)
XLA Ops:
  6.5 0.0 copy-start
  6.5 0.0 copy-start.4
  6.5 0.0 all-gather.5.cloned.1.call-start
  6.5 1.1 fusion.34
  7.7 0.9 fusion.36
  8.6 1.5 pad_maximum_fusion
  10.1 0.0 all-gather.5.cloned.1.call-update
  10.2 0.0 reduce-scatter.3.cloned.1.call-start
  10.2 0.7 convert_element_type.80
  10.9 0.5 slice.7
  11.4 13.5 %all-gather.1 = f32[8,1,256]{2,1,0:T(1,128)S(1)} all-gather(f32[1,1,256]{2,1,0:T(1,128)S(1)} %bitcast.73), channel_id=2, replica_groups=mesh['grp'=1,'sp'=8,'tp'=4] {'sp'}, dimensions={0}, use_global_device_ids=true | all-gather | bytes 9216 | tf_op jit(solution)/shard_map/all_gather | solution.py:42
  24.9 14.2 %all_gather.14 = f32[4,2048]{1,0:T(4,128)S(1)} all-gather(f32[4,256]{1,0:T(4,128)} %param.22), channel_id=1, replica_groups=mesh['grp'=1,'sp'=8,'tp'=4] {'sp'}, dimensions={1}, use_global_device_ids=true | all-gather | bytes 36864 | tf_op jit(solution)/shard_map/all_gather | solution.py:41
  39.1 1.2 fusion.23
  40.3 1.2 fusion.26
  41.5 0.0 all-gather.5.cloned.1.call-done
  41.5 2.1 fusion.50
  43.6 0.0 copy-done.4
  43.7 15.3 %while.15 = (s32[]{:T(128)}, f32[4,256]{1,0:T(4,128)S(1)}, f32[4,256]{1,0:T(4,128)S(1)}, f32[4,256,128]{2,1,0:T(8,128)S(1)}, s32[4]{0:T(128)S(1)}, /*index=5*/s3...) while((s32[]{:T(128)}, f32[4,256]{1,0:T(4,128)S(1)}, ...), condition=%wide.region_7.8_spmd.clone, body=%wide.region_2.7_spmd.clone.sunk | while | flops 273287936 | bytes 8237029 | solution.py:97
  43.7 0.6 dynamic_slice.48
  44.9 0.6 constant_dynamic-slice_fusion.5
  46.7 2.9 conditional.3
  46.8 0.1 constant_dynamic-slice_fusion
  46.9 0.2 compare_and_fusion
  47.1 1.5 fusion.49
  48.5 0.3 fusion.5
  48.9 0.7 convolution_add_fusion
  49.6 0.6 dynamic_slice.48
  50.9 0.6 constant_dynamic-slice_fusion.5
  52.7 0.6 dynamic_slice.48
  54.0 0.6 constant_dynamic-slice_fusion.5
  55.8 0.6 dynamic_slice.48
  57.1 0.6 constant_dynamic-slice_fusion.5
  58.9 0.2 copy.38
  59.2 0.0 copy-start.5
  59.2 0.0 copy-start.6
  59.2 0.0 copy-start.1
  59.2 0.0 copy-start.3
  59.2 3.4 convolution_convert_fusion.1
  62.6 0.0 reduce-scatter.3.cloned.1.call-update
  62.6 0.0 all-gather.7.cloned.1.call-start
  62.7 0.0 copy-done.5
  62.7 0.0 copy-done.6
  62.7 0.1 copy.39
  62.8 0.1 reduce_window_sum.11
  62.9 0.1 copy.40
  63.0 34.3 %reduce-scatter.3.cloned.1.call-done = bf16[64,2048]{1,0:T(8,128)(2,1)} async-done(((bf16[256,2048]{1,0:T(8,128)(2,1)}), bf16[64,2048]{1,0:T(8,128)(2,1)}) %reduce-scatter.3.cloned.1.call-update) | async-done | bytes 262160 | tf_op jit(solution)/shard_map/reduce_scatter | solution.py:104
  97.3 0.0 copy-done.1
  97.3 1.1 fusion.27
  98.5 0.0 copy-done.3
  98.5 1.4 convolution_convert_fusion.2
  99.9 0.2 broadcast_in_dim.72
  100.0 42.3 %all_to_all.10 = bf16[8,48,2048]{2,1,0:T(8,128)(2,1)} all-to-all(bf16[8,48,2048]{2,1,0:T(8,128)(2,1)S(1)} %bitcast.69), channel_id=1, replica_groups=mesh['grp'=1,'sp'=8,'tp'=4] {'sp'}, dimensions={0} | all-to-all | bytes 3145728 | tf_op jit(solution)/shard_map/all_to_all | solution.py:132
  142.4 0.0 all-gather.7.cloned.1.call-update
  142.4 0.0 reduce-scatter.5.cloned.1.call-start
  142.4 68.1 %all-gather.7.cloned.1.call-done = bf16[32,48,2048]{2,1,0:T(8,128)(2,1)} async-done(((bf16[8,48,2048]{2,1,0:T(8,128)(2,1)}), bf16[32,48,2048]{2,1,0:T(8,128)(2,1)}) %all-gather.7.cloned.1.call-update) | async-done | bytes 6291472 | tf_op jit(solution)/shard_map/all_gather | solution.py:131
  210.5 8.5 %fusion.19 = f32[1536,512]{1,0:T(8,128)} fusion(bf16[1536,2048]{1,0:T(8,128)(2,1)} %bitcast.78, bf16[1,2048,512]{2,1,0:T(8,128)(2,1)} %param.31), kind=kOutput, calls=%fused_computation.34 | convolution fusion | flops 3221225472 | bytes 11534336 | tf_op jit(solution)/shard_map/dot_general | solution.py:139
  219.0 0.0 copy-done
  219.0 11.7 %convolution_convert_fusion = bf16[1536,2048]{1,0:T(8,128)(2,1)} fusion(bf16[1,512,2048]{2,1,0:T(8,128)(2,1)S(1)} %copy-done, bf16[1536,2048]{1,0:T(8,128)(2,1)} %bitcast.79, f32[1536,512]{1,0:T(8,128)} %fusion.19, bf16[1,2048,512]{2,1,0:T(8,128)(2,1)} %param.32), kind=kOutput, calls=%fused_computation.23 | convolution fusion | flops 6450315264 | bytes 19922944 | tf_op jit(solution)/shard_map/dot_general | solution.py:142
  230.8 0.0 reduce-scatter.5.cloned.1.call-update
  230.8 70.2 %reduce-scatter.5.cloned.1.call-done = bf16[8,48,2048]{2,1,0:T(8,128)(2,1)} async-done(((bf16[32,48,2048]{2,1,0:T(8,128)(2,1)}), bf16[8,48,2048]{2,1,0:T(8,128)(2,1)}) %reduce-scatter.5.cloned.1.call-update) | async-done | bytes 1572880 | tf_op jit(solution)/shard_map/reduce_scatter | solution.py:146
  301.0 42.4 %all_to_all.11 = bf16[8,48,2048]{2,1,0:T(8,128)(2,1)S(1)} all-to-all(bf16[8,48,2048]{2,1,0:T(8,128)(2,1)} %reduce-scatter.5.cloned.1.call-done), channel_id=1, replica_groups=mesh['grp'=1,'sp'=8,'tp'=4] {'sp'}, dimensions={0} | all-to-all | bytes 3145728 | tf_op jit(solution)/shard_map/all_to_all | solution.py:149
  343.4 0.3 convert_reduce_fusion
  343.8 0.6 copy-done.2
  344.4 1.9 fusion.16
  (28 shorter events, 0.3 us)
Async XLA Ops:
  6.5 212.5 %copy-start = (bf16[1,512,2048]{2,1,0:T(8,128)(2,1)S(1)}, bf16[1,512,2048]{2,1,0:T(8,128)(2,1)}, u32[]{:S(2)}) copy-start(bf16[1,512,2048]{2,1,0:T(8,128)(2,1)} %param.33) | copy-start | bytes 6291460
  6.5 37.1 %copy-start.4 = (f32[4,256]{1,0:T(4,128)S(1)}, f32[4,256]{1,0:T(4,128)}, u32[]{:S(2)}) copy-start(f32[4,256]{1,0:T(4,128)} %param.22) | copy-start | bytes 12292
  6.5 35.0 %all-gather.5.cloned.1.call-start = ((), (), s32[]{:S(2)}) async-start(), calls=%async_computation.4 | async-start | bytes 1179648 | tf_op jit(solution)/shard_map/all_gather | solution.py:53
  10.2 87.1 %reduce-scatter.3.cloned.1.call-start = ((), (), s32[]{:S(2)}) async-start(), calls=%async_computation.5 | async-start | bytes 1310720 | tf_op jit(solution)/shard_map/reduce_scatter | solution.py:104
  59.2 3.5 copy-start.5
  59.2 3.5 copy-start.6
  59.2 38.1 %copy-start.1 = (bf16[64,2048]{1,0:T(8,128)(2,1)S(1)}, bf16[64,2048]{1,0:T(8,128)(2,1)}, u32[]{:S(2)}) copy-start(bf16[64,2048]{1,0:T(8,128)(2,1)} %param.27) | copy-start | bytes 786436
  59.2 39.2 %copy-start.3 = (f32[2048]{0:T(1024)S(1)}, f32[2048]{0:T(1024)}, u32[]{:S(2)}) copy-start(f32[2048]{0:T(1024)} %param.28) | copy-start | bytes 24580
  62.6 147.9 %all-gather.7.cloned.1.call-start = ((), (), s32[]{:S(2)}) async-start(), calls=%async_computation.6 | async-start | bytes 7864320 | tf_op jit(solution)/shard_map/all_gather | solution.py:131
  142.4 158.6 %reduce-scatter.5.cloned.1.call-start = ((), (), s32[]{:S(2)}) async-start(), calls=%async_computation.7 | async-start | bytes 7864320 | tf_op jit(solution)/shard_map/reduce_scatter | solution.py:146
  343.4 1.0 copy-start.2
Sparse Core Ops, SparseCore 0:
  10.3 24.9 all-gather.4
  62.7 34.5 reduce-scatter.2
  142.5 67.9 all-gather.6
  230.9 70.0 reduce-scatter.4
